TPU v7x, 32 devices: a whole 2x2x4 slice. The times are simulated.
32 devices in a mesh: sp: 8 (over z, x), tp: 4 (over y, core).
Axes of the slice: x: 2, y: 2, z: 4, core: 2. Of those that a mesh axis runs over, the one named last changes fastest.
Arguments:
- residual: bfloat16 [2048, 2048], P(('sp', 'tp')), may hold values from -6 to 6
- first_query: bfloat16 [2048, 512], P('sp', 'tp'), may hold values from -6 to 6
- second_query: bfloat16 [2048, 512], P('sp', 'tp'), may hold values from -6 to 6
- first_key: bfloat16 [2048, 512], P('sp', 'tp'), may hold values from -6 to 6
- second_key: bfloat16 [2048, 512], P('sp', 'tp'), may hold values from -6 to 6
- values: bfloat16 [2048, 1024], P('sp', 'tp'), may hold values from -6 to 6
- lambdas: float32 [8], P('tp'), may hold values from 0.3 to 0.8
- head_gain: float32 [128], replicated, may hold values from 0.1 to 1.9
- out_weight: bfloat16 [1024, 2048], P('tp'), may hold values from -0.1875 to 0.1875
- norm_gain: float32 [2048], replicated, may hold values from 0.1 to 1.9
- up_weight: bfloat16 [2048, 4096], P('sp', 'tp'), may hold values from -0.125 to 0.125
- down_weight: bfloat16 [4096, 2048], P('tp', 'sp'), may hold values from -0.09375 to 0.09375
Outputs:
- mixed: bfloat16 [2048, 2048], P(('sp', 'tp'))
All inputs are finite; a program needn't handle non-finite values.
Results may differ from a plain program's by a relative error of at most 0.019.
Values may be sent and summed in bfloat16 or wider, within the bound.
A program may use at most 128 MiB of HBM per device.

v0:
```python
import functools

import jax
import jax.numpy as jnp
import numpy as np
from jax import lax
from jax.experimental import pallas as pl
from jax.experimental.pallas import tpu as pltpu
from jax.sharding import PartitionSpec as P


def rotate(blocked, positions):
    half = blocked.shape[-1] // 2
    inverse = 10000.0 ** (-jnp.arange(0, half, dtype=jnp.float32) * 2.0 / blocked.shape[-1])
    angle = positions[:, None] * inverse[None, :]
    cosine = jnp.cos(angle)[:, None, :]
    sine = jnp.sin(angle)[:, None, :]
    first, second = (blocked[..., :half], blocked[..., half:])
    return jnp.concatenate(
        [first * cosine - second * sine, second * cosine + first * sine], axis=-1
    )


def absorb(state, queries, keys, vals, factor):
    top, total, summed = state
    scores = jnp.einsum("qhe,khe->qhk", queries, keys, preferred_element_type=jnp.float32) * factor
    peak = jnp.maximum(top, jnp.max(scores, axis=-1))
    shrink = jnp.exp(top - peak)
    weights = jnp.exp(scores - peak[..., None])
    total = total * shrink + jnp.sum(weights, axis=-1)
    summed = summed * shrink[..., None] + jnp.einsum(
        "qhk,khe->qhe", weights.astype(jnp.bfloat16), vals, preferred_element_type=jnp.float32
    )
    return (peak, total, summed)


def layer_norm(stream, gain):
    center = stream - jnp.mean(stream, axis=-1, keepdims=True)
    spread = jnp.mean(center * center, axis=-1, keepdims=True)
    return center * lax.rsqrt(spread + 1e-05) * gain


def local(
    residual,
    first_query,
    second_query,
    first_key,
    second_key,
    values,
    lambdas,
    head_gain,
    out_weight,
    norm_gain,
    up_weight,
    down_weight,
):
    local_rows = first_query.shape[0]
    head_count = lambdas.shape[0]
    head_width = first_query.shape[1] // head_count
    value_width = values.shape[1] // head_count
    quarter_rows = local_rows // lax.axis_size("tp")
    factor = head_width ** (-0.5)
    positions = (lax.axis_index("sp") * local_rows + jnp.arange(local_rows)).astype(jnp.float32)

    def prepare(source):
        turned = rotate(
            source.astype(jnp.float32).reshape(local_rows, head_count, head_width), positions
        )
        return turned.astype(jnp.bfloat16)

    query_a, query_b = (prepare(first_query), prepare(second_query))
    key_a = prepare(first_key).reshape(local_rows, head_count * head_width)
    key_b = prepare(second_key).reshape(local_rows, head_count * head_width)
    start_state = (
        jnp.full((local_rows, head_count), -1e30, jnp.float32),
        jnp.zeros((local_rows, head_count), jnp.float32),
        jnp.zeros((local_rows, head_count, value_width), jnp.float32),
    )
    piece_a = lax.all_gather(key_a, "sp", axis=0, tiled=True)
    piece_b = lax.all_gather(key_b, "sp", axis=0, tiled=True)
    piece_v = lax.all_gather(values, "sp", axis=0, tiled=True)
    count = piece_a.shape[0]
    block = 512
    blocks = count // block

    def advance(state, item):
        block_a, block_b, block_v = item
        return (
            (
                absorb(state[0], query_a, block_a, block_v, factor),
                absorb(state[1], query_b, block_b, block_v, factor),
            ),
            None,
        )

    items = (
        piece_a.reshape(blocks, block, head_count, head_width),
        piece_b.reshape(blocks, block, head_count, head_width),
        piece_v.reshape(blocks, block, head_count, value_width),
    )
    state_a, state_b = lax.scan(advance, (start_state, start_state), items)[0]
    diff = state_a[2] / state_a[1][..., None] - lambdas[None, :, None] * (
        state_b[2] / state_b[1][..., None]
    )
    scale = lax.rsqrt(jnp.mean(diff * diff, axis=-1, keepdims=True) + 1e-05)
    flat = (
        (diff * scale * head_gain * 0.8)
        .astype(jnp.bfloat16)
        .reshape(local_rows, head_count * value_width)
    )
    projected = lax.psum(
        jnp.dot(flat, out_weight, preferred_element_type=jnp.float32).astype(jnp.bfloat16), "tp"
    ).astype(jnp.float32)
    stream = lax.all_gather(residual, "tp", axis=0, tiled=True)
    whole = layer_norm(stream.astype(jnp.float32) + projected, norm_gain).astype(jnp.bfloat16)
    own_normed = lax.dynamic_slice_in_dim(
        whole, lax.axis_index("tp") * quarter_rows, quarter_rows, 0
    )
    lifted = jnp.dot(
        whole,
        lax.all_gather(up_weight, "sp", axis=0, tiled=True),
        preferred_element_type=jnp.float32,
    )
    down_full = lax.all_gather(down_weight, "sp", axis=1, tiled=True)
    hidden = jnp.square(jax.nn.relu(lifted)).astype(jnp.bfloat16)
    lowered = lax.psum_scatter(
        jnp.dot(hidden, down_full, preferred_element_type=jnp.float32).astype(jnp.bfloat16),
        "tp",
        scatter_dimension=0,
        tiled=True,
    ).astype(jnp.float32)
    return (own_normed.astype(jnp.float32) + lowered).astype(jnp.bfloat16)


BF = jnp.bfloat16
F32 = jnp.float32
VMEM_BUDGET = 40 * 2**20


def layer_kernel(
    n, nt, heads,
    qa_far, qb_far, ka_far, kb_far, v_far, inverse, lam, hgain, ow0, res0, ngain, up0, dn0,
    out,
    qm, kv0, kv, up, dn, ow, res, flat, normed, lifted, hidden, part, mine, got,
    top, total, summed, send, recv, load, qa, qb, ka, kb,
):
    s = lax.axis_index("sp")
    t = lax.axis_index("tp")
    rows, kv_width = kv0.shape
    width = qm.shape[2]
    value_width = (kv_width - 2 * width) // heads
    depth = up0.shape[0]
    units = up0.shape[1]
    model = ow0.shape[1]
    piece = res0.shape[0]
    mid = n // 2
    odd = s % 2
    place = (1 - odd) * (s // 2) + odd * (n - 1 - s // 2)

    def at_place(p):
        p = p % n
        hi = p // mid
        return (1 - hi) * (2 * p) + hi * (2 * (n - 1 - p) + 1)

    def owner(slot):
        return at_place(place - slot + n)

    right = {"sp": at_place(place + 1)}
    left = {"sp": at_place(place + n - 1)}
    mates = [{"tp": (t + d) % nt} for d in range(1, nt)]
    loads = [
        pltpu.make_async_copy(src, dst, load.at[i])
        for i, (src, dst) in enumerate(((up0, up.at[0]), (dn0, dn.at[0]), (ow0, ow.at[t])))
    ]
    entries = [
        pltpu.make_async_copy(src, dst, load.at[3 + i])
        for i, (src, dst) in enumerate((
            (ka_far, ka), (kb_far, kb), (v_far, kv0.at[:, pl.ds(2 * width, v_far.shape[1])]),
            (qa_far, qa), (qb_far, qb),
        ))
    ]
    for c in entries + loads:
        c.start()
    barrier = pltpu.get_barrier_semaphore()
    for peer in [right, left] + mates:
        pl.semaphore_signal(barrier, inc=1, device_id=peer, device_id_type=pl.DeviceIdType.MESH)
    pl.semaphore_wait(barrier, nt + 1)

    copies = []

    def remote(src, dst, peer):
        i = len(copies)
        c = pltpu.make_async_remote_copy(
            src_ref=src, dst_ref=dst, send_sem=send.at[i], recv_sem=recv.at[i],
            device_id=peer, device_id_type=pl.DeviceIdType.MESH,
        )
        c.start()
        copies.append(c)
        return c

    own_of = {"kv": (kv0, kv), "up": (up0, up), "dn": (dn0, dn)}
    groups = {}

    def issue(name, k, *which):
        own, buf = own_of[name]
        size = own.shape[0]
        for i in which:
            if k > 1:
                ready(name, k - 1, i)
            a = pl.ds(i * (size // 2), size // 2)
            b = pl.ds((1 - i) * (size // 2), size // 2)
            src_a = own.at[a] if k == 1 else buf.at[k - 1, a]
            src_b = own.at[b] if k == 1 else buf.at[n - k + 1, b]
            groups[name, k, i] = [
                remote(src_a, buf.at[k, a], right),
                remote(src_b, buf.at[n - k, b], left),
            ]

    def ready(name, k, *which):
        for i in which:
            arrive(groups[name, k, i])
            groups[name, k, i] = []

    def arrive(group):
        for c in group:
            c.wait_recv()

    def absorb(block):
        for which in range(2):
            keys = block[:, which * width : (which + 1) * width]
            for h in range(heads):
                at = which * heads + h
                scores = lax.dot_general(
                    keys, qm[which, h * rows : (h + 1) * rows, :],
                    (((1,), (1,)), ((), ())), preferred_element_type=F32,
                )
                old = top[at]
                peak = jnp.maximum(old, jnp.max(scores, axis=0, keepdims=True))
                shrink = jnp.exp(old - peak)
                e = jnp.exp(scores - peak)
                top[at] = peak
                total[at] = total[at] * shrink + jnp.sum(e, axis=0, keepdims=True)
                first = 2 * width + h * value_width
                vals = block[:, first : first + value_width]
                summed[at] = summed[at] * shrink + lax.dot_general(
                    vals, e.astype(BF), (((0,), (0,)), ((), ())), preferred_element_type=F32
                )

    def absorb_pair(k):
        def body(i, carry):
            absorb(kv[k + i * (n - 2 * k)])
            return carry

        lax.fori_loop(0, 2, body, 0)

    partner = {"tp": t + 1 - 2 * (t % 2)}
    issue("up", 1, 0)
    across = range(2, nt, 2)
    far = [
        (d, [remote(res0, res.at[t], {"tp": (t + d) % nt}), remote(ow0, ow.at[t], {"tp": (t + d) % nt})])
        for d in across
    ]
    near = [remote(res0, res.at[t], partner), remote(ow0, ow.at[t], partner)]
    head_width = width // heads
    half = head_width // 2
    lane = lax.broadcasted_iota(jnp.int32, (rows, width), 1)
    low = (lane % head_width) < half
    position = (lax.broadcasted_iota(jnp.int32, (rows, width), 0) + s * rows).astype(F32)
    angle = position * inverse[...]
    cos = jnp.cos(angle)
    sin = jnp.sin(angle)
    sin = jnp.where(low, -sin, sin)

    def turn(ref):
        x = ref[...].astype(F32)
        other = jnp.where(low, pltpu.roll(x, width - half, 1), pltpu.roll(x, half, 1))
        return x * cos + other * sin

    for c in entries:
        c.wait()
    kv0[:, :width] = turn(ka).astype(BF)
    kv0[:, width : 2 * width] = turn(kb).astype(BF)
    for which, ref in enumerate((qa, qb)):
        q = turn(ref).astype(BF).astype(F32) * head_width ** (-0.5)
        for h in range(heads):
            own = (lane // head_width) == h
            qm[which, h * rows : (h + 1) * rows, :] = jnp.where(own, q, 0.0).astype(BF)
    issue("kv", 1, 0, 1)
    issue("up", 1, 1)
    top[...] = jnp.full(top.shape, -1e30, F32)
    total[...] = jnp.zeros(total.shape, F32)
    summed[...] = jnp.zeros(summed.shape, F32)
    res[t] = res0[...]
    absorb(kv0[...])
    fillers = [("dn", 1, 0), ("dn", 1, 1), ("up", 2, 0, 1)]
    for k in range(1, mid):
        issue("kv", k + 1, 0)
        ready("kv", k, 1)
        if k + 1 < mid:
            issue("kv", k + 1, 1)
        if fillers:
            issue(*fillers.pop(0))
        absorb_pair(k)
    for filler in fillers:
        issue(*filler)
    ready("kv", mid, 0)
    issue("dn", 2, 0, 1)
    absorb(kv[mid])

    for h in range(heads):
        a = summed[h] / total[h]
        b = summed[heads + h] / total[heads + h]
        diff = a - lam[h] * b
        scale = lax.rsqrt(jnp.mean(diff * diff, axis=0, keepdims=True) + 1e-05)
        done = (diff * scale).T * hgain[...] * 0.8
        flat[0, :, h * value_width : (h + 1) * value_width] = done.astype(BF)

    got_flat = [remote(flat.at[0], flat.at[d + 1], m) for d, m in enumerate(mates)]
    for d, pair in far:
        arrive(pair)
        there = (t + nt - d) % nt
        near += [remote(res.at[there], res.at[there], partner), remote(ow.at[there], ow.at[there], partner)]
    arrive(near + got_flat)
    for c in loads:
        c.wait()

    chunk = piece
    def norm_rows(q, carry):
        rows_at = pl.ds(pl.multiple_of(q * chunk, chunk), chunk)
        stream = res[q].astype(F32) + jnp.dot(flat[0, rows_at, :], ow[t], preferred_element_type=F32)
        for d in range(1, nt):
            stream += jnp.dot(flat[d, rows_at, :], ow[(t + nt - d) % nt], preferred_element_type=F32)
        center = stream - jnp.mean(stream, axis=-1, keepdims=True)
        spread = jnp.mean(center * center, axis=-1, keepdims=True)
        row = (center * lax.rsqrt(spread + 1e-05) * ngain[...]).astype(BF)
        for i in range(n):
            normed[i, q] = row[:, i * depth : (i + 1) * depth]
        return carry

    lax.fori_loop(0, nt, norm_rows, 0)

    def lift(block, slot):
        x = normed[owner(slot)].reshape(rows, depth)
        return jnp.dot(x, block, preferred_element_type=F32)

    def lift_pair(k):
        def body(i, carry):
            slot = k + i * (n - 2 * k)
            lifted[...] += lift(up[slot], slot)
            return carry

        lax.fori_loop(0, 2, body, 0)

    lifted[...] = lift(up[0], 0)
    ready("up", 1, 0, 1)
    lift_pair(1)
    for k in range(2, mid):
        issue("up", k + 1, 0)
        if k + 1 < mid:
            issue("up", k + 1, 1)
        if k > 2:
            issue("dn", k, 0, 1)
        ready("up", k, 1)
        lift_pair(k)
    ready("up", mid, 0)
    h = jnp.maximum(lifted[...] + lift(up[mid], mid), 0.0)
    hidden[...] = (h * h).astype(BF)

    waits = []

    def lower(block, slot):
        y = jnp.dot(hidden[...], block, preferred_element_type=F32).reshape(nt, piece, depth)
        mine[slot] = y
        part[slot] = y.astype(BF)

    def share(slot):
        waits.append((slot, [
            remote(part.at[slot, (t + d) % nt], got.at[slot, d - 1], mates[d - 1])
            for d in range(1, nt)
        ]))

    def finish(slot, group):
        arrive(group)
        who = owner(slot)
        y = normed[who, t].astype(F32) + mine[slot, t]
        for d in range(nt - 1):
            y += got[slot, d].astype(F32)
        out[:, pl.ds(pl.multiple_of(who * depth, depth), depth)] = y.astype(BF)

    lower(dn[0], 0)
    ready("dn", 1, 0, 1)
    last = 0
    for k in range(1, mid):
        if k == mid - 1:
            issue("dn", mid, 0)
        ready("dn", k, 0, 1)
        for slot in (k, n - k):
            lower(dn[slot], slot)
            share(last)
            last = slot
    share(last)
    for slot, group in waits[:-2]:
        finish(slot, group)
    ready("dn", mid, 0)
    lower(dn[mid], mid)
    for slot, group in waits[-2:]:
        finish(slot, group)
    share(mid)
    finish(*waits[-1])
    for c in copies:
        c.wait_send()


def fused(n, nt, residual, first_query, second_query, first_key, second_key, values,
          lambdas, head_gain, out_weight, norm_gain, up_weight, down_weight):
    rows, width = first_query.shape
    heads = lambdas.shape[0]
    head_width = width // heads
    value_width = values.shape[1] // heads
    half = head_width // 2
    depth, units = up_weight.shape
    model = out_weight.shape[1]
    piece = residual.shape[0]
    inverse = 10000.0 ** (-np.arange(half) * 2.0 / head_width)
    inverse = np.tile(inverse, 2 * heads)[None, :].astype(np.float32)
    kv_width = 2 * width + heads * value_width
    vmem = pl.BlockSpec(memory_space=pltpu.VMEM)
    smem = pl.BlockSpec(memory_space=pltpu.SMEM)
    far = pl.BlockSpec(memory_space=pl.ANY)
    mid = n // 2
    count = 6 * (n - 1) + 3 * nt + (n + 1) * (nt - 1)
    maps = 2 * heads
    return pl.pallas_call(
        functools.partial(layer_kernel, n, nt, heads),
        out_shape=jax.ShapeDtypeStruct((piece, model), BF),
        in_specs=[far] * 5 + [vmem, smem, vmem, far, vmem, vmem, far, far],
        out_specs=vmem,
        scratch_shapes=[
            pltpu.VMEM((2, heads * rows, width), BF),
            pltpu.VMEM((rows, kv_width), BF),
            pltpu.VMEM((n, rows, kv_width), BF),
            pltpu.VMEM((n, depth, units), BF),
            pltpu.VMEM((n, units, depth), BF),
            pltpu.VMEM((nt,) + out_weight.shape, BF),
            pltpu.VMEM((nt, piece, model), BF),
            pltpu.VMEM((nt, rows, heads * value_width), BF),
            pltpu.VMEM((n, nt, piece, depth), BF),
            pltpu.VMEM((rows, units), F32),
            pltpu.VMEM((rows, units), BF),
            pltpu.VMEM((n, nt, piece, depth), BF),
            pltpu.VMEM((n, nt, piece, depth), F32),
            pltpu.VMEM((n, nt - 1, piece, depth), BF),
            pltpu.VMEM((maps, 1, rows), F32),
            pltpu.VMEM((maps, 1, rows), F32),
            pltpu.VMEM((maps, value_width, rows), F32),
            pltpu.SemaphoreType.DMA((count,)),
            pltpu.SemaphoreType.DMA((count,)),
            pltpu.SemaphoreType.DMA((8,)),
        ] + [pltpu.VMEM((rows, width), BF)] * 4,
        compiler_params=pltpu.CompilerParams(
            collective_id=0, has_side_effects=True, vmem_limit_bytes=60 * 2**20
        ),
        name="layer",
    )(first_query, second_query, first_key, second_key, values, inverse,
      lambdas, head_gain.reshape(1, -1), out_weight, residual,
      norm_gain.reshape(1, -1), up_weight, down_weight)


def choose(*args):
    n, nt = lax.axis_size("sp"), lax.axis_size("tp")
    gathered = n * sum(a.size * a.dtype.itemsize for a in (args[3], args[4], args[5], args[10], args[11]))
    gathered += nt * sum(a.size * a.dtype.itemsize for a in (args[0], args[8]))
    if n % 2 == 0 and n >= 6 and nt % 2 == 0 and 2 * gathered <= VMEM_BUDGET:
        return fused(n, nt, *args)
    return local(*args)


def solution(mesh):
    in_specs = (
        P(("sp", "tp"), None),
        P("sp", "tp"),
        P("sp", "tp"),
        P("sp", "tp"),
        P("sp", "tp"),
        P("sp", "tp"),
        P("tp"),
        P(),
        P("tp", None),
        P(),
        P("sp", "tp"),
        P("tp", "sp"),
    )
    out_specs = P(("sp", "tp"), None)
    return jax.shard_map(choose, mesh=mesh, in_specs=in_specs, out_specs=out_specs, check_vma=False)
```

profile of v0, /device:TPU:0, one launch (start us, length us, event | category | flops | bytes accessed | tf_op | source)
XLA Modules:
  0.0 112.5 jit_solution(12787389020220801517)
XLA Ops:
  0.0 110.9 %layer.1 = bf16[64,2048]{1,0:T(8,128)(2,1)} custom-call(bf16[256,128]{1,0:T(8,128)(2,1)} %qa_far.1, bf16[256,128]{1,0:T(8,128)(2,1)} %qb_far.1, bf16[256,128]{1,0:T(8,128)(2,1)} %ka_far.1, bf16[256,128]{1,0:T(8,128)(2,1)} %kb_far.1, bf16[256,256]{1,0:T(8,128)(2,1)} %v_far.1, f32[1,128]{1,0:T(1,128)} %constant.2.clone.inverse, f32[2]{0:T(128)} %lam.1, ...), custom_call_target="tpu_custom_call" | custom-call | tf_op jit(solution)/shard_map/layer/pallas_call | solution.py:433
  110.9 1.7 %copy.15 = bf16[64,2048]{1,0:T(8,128)(2,1)} copy(bf16[64,2048]{1,0:T(8,128)(2,1)} %layer.1) | data formatting | bytes 524288
where the time goes:
time: 113 us
  Pallas kernels  111 us (98%)
  local copies, waits for them, and re-layouts  1.67 us (1%)
    pallas_call x1, Pallas kernels, fused(): pl.pallas_call(functools.partial(layer_kernel, n, nt, heads), out_shape=j...  111 us

commit v1 on v0

v1 whole, which is shorter than its diff:
```python
import functools

import jax
import jax.numpy as jnp
import numpy as np
from jax import lax
from jax.experimental import pallas as pl
from jax.experimental.pallas import tpu as pltpu
from jax.sharding import PartitionSpec as P


def rotate(blocked, positions):
    half = blocked.shape[-1] // 2
    inverse = 10000.0 ** (-jnp.arange(0, half, dtype=jnp.float32) * 2.0 / blocked.shape[-1])
    angle = positions[:, None] * inverse[None, :]
    cosine = jnp.cos(angle)[:, None, :]
    sine = jnp.sin(angle)[:, None, :]
    first, second = (blocked[..., :half], blocked[..., half:])
    return jnp.concatenate(
        [first * cosine - second * sine, second * cosine + first * sine], axis=-1
    )


def absorb(state, queries, keys, vals, factor):
    top, total, summed = state
    scores = jnp.einsum("qhe,khe->qhk", queries, keys, preferred_element_type=jnp.float32) * factor
    peak = jnp.maximum(top, jnp.max(scores, axis=-1))
    shrink = jnp.exp(top - peak)
    weights = jnp.exp(scores - peak[..., None])
    total = total * shrink + jnp.sum(weights, axis=-1)
    summed = summed * shrink[..., None] + jnp.einsum(
        "qhk,khe->qhe", weights.astype(jnp.bfloat16), vals, preferred_element_type=jnp.float32
    )
    return (peak, total, summed)


def layer_norm(stream, gain):
    center = stream - jnp.mean(stream, axis=-1, keepdims=True)
    spread = jnp.mean(center * center, axis=-1, keepdims=True)
    return center * lax.rsqrt(spread + 1e-05) * gain


def local(
    residual,
    first_query,
    second_query,
    first_key,
    second_key,
    values,
    lambdas,
    head_gain,
    out_weight,
    norm_gain,
    up_weight,
    down_weight,
):
    local_rows = first_query.shape[0]
    head_count = lambdas.shape[0]
    head_width = first_query.shape[1] // head_count
    value_width = values.shape[1] // head_count
    quarter_rows = local_rows // lax.axis_size("tp")
    factor = head_width ** (-0.5)
    positions = (lax.axis_index("sp") * local_rows + jnp.arange(local_rows)).astype(jnp.float32)

    def prepare(source):
        turned = rotate(
            source.astype(jnp.float32).reshape(local_rows, head_count, head_width), positions
        )
        return turned.astype(jnp.bfloat16)

    query_a, query_b = (prepare(first_query), prepare(second_query))
    key_a = prepare(first_key).reshape(local_rows, head_count * head_width)
    key_b = prepare(second_key).reshape(local_rows, head_count * head_width)
    start_state = (
        jnp.full((local_rows, head_count), -1e30, jnp.float32),
        jnp.zeros((local_rows, head_count), jnp.float32),
        jnp.zeros((local_rows, head_count, value_width), jnp.float32),
    )
    piece_a = lax.all_gather(key_a, "sp", axis=0, tiled=True)
    piece_b = lax.all_gather(key_b, "sp", axis=0, tiled=True)
    piece_v = lax.all_gather(values, "sp", axis=0, tiled=True)
    count = piece_a.shape[0]
    block = 512
    blocks = count // block

    def advance(state, item):
        block_a, block_b, block_v = item
        return (
            (
                absorb(state[0], query_a, block_a, block_v, factor),
                absorb(state[1], query_b, block_b, block_v, factor),
            ),
            None,
        )

    items = (
        piece_a.reshape(blocks, block, head_count, head_width),
        piece_b.reshape(blocks, block, head_count, head_width),
        piece_v.reshape(blocks, block, head_count, value_width),
    )
    state_a, state_b = lax.scan(advance, (start_state, start_state), items)[0]
    diff = state_a[2] / state_a[1][..., None] - lambdas[None, :, None] * (
        state_b[2] / state_b[1][..., None]
    )
    scale = lax.rsqrt(jnp.mean(diff * diff, axis=-1, keepdims=True) + 1e-05)
    flat = (
        (diff * scale * head_gain * 0.8)
        .astype(jnp.bfloat16)
        .reshape(local_rows, head_count * value_width)
    )
    projected = lax.psum(
        jnp.dot(flat, out_weight, preferred_element_type=jnp.float32).astype(jnp.bfloat16), "tp"
    ).astype(jnp.float32)
    stream = lax.all_gather(residual, "tp", axis=0, tiled=True)
    whole = layer_norm(stream.astype(jnp.float32) + projected, norm_gain).astype(jnp.bfloat16)
    own_normed = lax.dynamic_slice_in_dim(
        whole, lax.axis_index("tp") * quarter_rows, quarter_rows, 0
    )
    lifted = jnp.dot(
        whole,
        lax.all_gather(up_weight, "sp", axis=0, tiled=True),
        preferred_element_type=jnp.float32,
    )
    down_full = lax.all_gather(down_weight, "sp", axis=1, tiled=True)
    hidden = jnp.square(jax.nn.relu(lifted)).astype(jnp.bfloat16)
    lowered = lax.psum_scatter(
        jnp.dot(hidden, down_full, preferred_element_type=jnp.float32).astype(jnp.bfloat16),
        "tp",
        scatter_dimension=0,
        tiled=True,
    ).astype(jnp.float32)
    return (own_normed.astype(jnp.float32) + lowered).astype(jnp.bfloat16)


BF = jnp.bfloat16
F32 = jnp.float32
VMEM_BUDGET = 40 * 2**20
PIECES = 2
MESH = pl.DeviceIdType.MESH


def receive_slots(nz):
    sizes = dict(kvz=nz, kvx=nz, kvs=nz, kvt=nz, q=nz, head=2 * nz, lam=1, ow=6, norm=6)
    for name in ("up", "dn"):
        for way in "zxst":
            sizes[name + way] = nz * PIECES
    sizes.update(yg=2 * nz * PIECES, zg=2 * nz * PIECES)
    base, at = {}, 0
    for name, size in sizes.items():
        base[name] = at
        at += size
    return base, at


def layer_kernel(
    nz, head_width,
    qa_far, qb_far, ka_far, kb_far, v_far, inverse, lam, hgain, ow0, res0, ngain, up0, dn0,
    out,
    kvs, qs, kv, qb, qm, lamt, hsrc, hb, up, dn, ow, nb, hidden, mine, part, ygot, zsend, zgot,
    top, total, summed, send, recv, load, qa, qbb, ka, kb,
):
    s = lax.axis_index("sp")
    t = lax.axis_index("tp")
    z, x, y, c = s // 2, s % 2, t // 2, t % 2
    zl = z % 2
    base, _ = receive_slots(nz)
    rows, width = ka.shape
    piece = res0.shape[0]
    depth = up0.shape[0]
    units = up0.shape[1]
    half_rows = rows // 2
    P_ = PIECES

    def dev(x_, y_, z_, c_):
        return {"sp": z_ * 2 + x_, "tp": y_ * 2 + c_}

    sib = dev(x, y, z, 1 - c)
    xnb = dev(1 - x, y, z, c)
    ynb = dev(x, 1 - y, z, c)
    znb = dev(x, y, z + 1 - 2 * zl, c)
    order = [z, z + 1 - 2 * zl, (z + 2) % nz, nz - 1 - z]

    loads = [
        pltpu.make_async_copy(src, dst, load.at[i])
        for i, (src, dst) in enumerate((
            (ka_far, ka), (kb_far, kb), (qa_far, qa), (qb_far, qbb),
            (v_far.at[:, :width], kvs.at[0, :, width:]), (v_far.at[:, width:], kvs.at[1, :, width:]),
            (ow0, ow.at[t]),
        ))
    ]
    for cp in loads:
        cp.start()
    barrier = pltpu.get_barrier_semaphore()
    peers = [xnb, sib]
    peers += [dev(x, y, (z + k) % nz, d) for k in range(1, nz) for d in range(2)]
    peers += [dev(x, 1 - y, (z + k) % nz, c) for k in range(nz)]
    for peer in peers:
        pl.semaphore_signal(barrier, inc=1, device_id=peer, device_id_type=MESH)

    started = []

    def remote(src, dst, slot, peer, unless=None, local=False):
        i = len(started)
        cp = pltpu.make_async_remote_copy(
            src_ref=src, dst_ref=dst, send_sem=send.at[i], recv_sem=recv.at[slot],
            device_id=peer, device_id_type=MESH,
        )
        started.append((cp, unless))
        if unless is None:
            cp.start()
        else:
            pl.when(jnp.logical_not(unless))(cp.start)
            if local:
                pl.when(unless)(pltpu.make_async_copy(src, dst, recv.at[slot]).start)

    def got(dst, slot, unless=None):
        cp = pltpu.make_async_remote_copy(
            src_ref=dst, dst_ref=dst, send_sem=send.at[0], recv_sem=recv.at[slot],
            device_id=sib, device_id_type=MESH,
        )
        if unless is None:
            cp.wait_recv()
        else:
            pl.when(jnp.logical_not(unless))(cp.wait_recv)

    def ow_half(ref, i):
        return ref.at[pl.ds(i * (rows // 2), rows // 2)]

    weights = {"up": (up0, up), "dn": (dn0, dn)}

    def spread(name, far, pieces=range(P_)):
        own, buf = weights[name]
        size = buf.shape[4]
        span = buf.shape[5]
        for p in pieces:
            for z_t in (c, c + 2):
                for d in range(2):
                    if name == "up":
                        src = own.at[pl.ds((d * P_ + p) * size, size)]
                    else:
                        src = own.at[pl.ds(d * size, size), pl.ds(p * span, span)]
                    dst = buf.at[x, z, p, d]
                    slot = base[name + "z"] + z * P_ + p
                    here = z_t == z
                    skip = here if far else jnp.logical_not(here)
                    if far:
                        remote(src, dst, slot, dev(x, y, z_t, d), unless=here)
                    else:
                        i = len(started)
                        cp = pltpu.make_async_remote_copy(
                            src_ref=src, dst_ref=dst, send_sem=send.at[i], recv_sem=recv.at[slot],
                            device_id=sib, device_id_type=MESH,
                        )
                        away = jnp.logical_or(skip, d == c)
                        started.append((cp, away))
                        pl.when(jnp.logical_not(away))(cp.start)
                        near = jnp.logical_and(here, d == c)
                        pl.when(near)(pltpu.make_async_copy(src, dst, recv.at[slot]).start)

    def relay_z(name, k, pieces=range(P_)):
        buf = weights[name][1]
        zz = order[k]
        for p in pieces:
            ref = buf.at[x, zz, p, c]
            got(ref, base[name + "z"] + zz * P_ + p)
            remote(ref, ref, base[name + "x"] + zz * P_ + p, xnb)
            remote(ref, ref, base[name + "s"] + zz * P_ + p, sib)

    def relay_x(name, k, pieces=range(P_)):
        buf = weights[name][1]
        zz = order[k]
        for p in pieces:
            ref = buf.at[1 - x, zz, p, c]
            got(ref, base[name + "x"] + zz * P_ + p)
            remote(ref, ref, base[name + "t"] + zz * P_ + p, sib)

    def settle(name, k, other, pieces=range(P_)):
        buf = weights[name][1]
        zz = order[k]
        for p in pieces:
            ref = buf.at[1 - x if other else x, zz, p, 1 - c]
            got(ref, base[name + ("t" if other else "s")] + zz * P_ + p)

    half = head_width // 2
    lane = lax.broadcasted_iota(jnp.int32, (rows, width), 1)
    low = (lane % head_width) < half
    front = lane < head_width
    position = (lax.broadcasted_iota(jnp.int32, (rows, width), 0) + s * rows).astype(F32)
    angle = position * inverse[...]
    cos = jnp.cos(angle)
    sin = jnp.sin(angle)
    sin = jnp.where(low, -sin, sin)

    def turn(ref):
        v = ref[...].astype(F32)
        other = jnp.where(low, pltpu.roll(v, width - half, 1), pltpu.roll(v, half, 1))
        return v * cos + other * sin

    def packed(a, b):
        first = jnp.where(front, a, pltpu.roll(b, head_width, 1))
        second = jnp.where(front, pltpu.roll(a, head_width, 1), b)
        return first.astype(BF), second.astype(BF)

    lamt[0] = jnp.full(lamt.shape[1:], lam[zl], F32)
    pl.semaphore_wait(barrier, len(peers))
    spread("up", False)
    for i in range(2):
        remote(ow_half(ow0, i), ow_half(ow.at[t], i), base["ow"] + 2 + i, ynb)
    for i in range(2):
        remote(ow_half(ow0, i), ow_half(ow.at[t], i), base["ow"] + i, sib)
    for cp in loads[:2]:
        cp.wait()
    for j, v in enumerate(packed(turn(ka), turn(kb))):
        kvs[j, :, :width] = v
    for cp in loads[4:6]:
        cp.wait()
    for j in range(2):
        z_t = 2 * c + j
        for d in range(2):
            remote(
                kvs.at[j, pl.ds(d * half_rows, half_rows)], kv.at[x, z, d], base["kvz"] + z,
                dev(x, y, z_t, d), unless=jnp.logical_and(z_t == z, d == c),
            )
    for cp in loads[2:4]:
        cp.wait()
    scale = head_width ** (-0.5)
    for j, v in enumerate(packed(turn(qa), turn(qbb))):
        qs[j] = (v.astype(F32) * scale).astype(BF).reshape(qs.shape[1:])
    for j in range(2):
        z_t = 2 * c + j
        for d in range(2):
            remote(
                qs.at[j, :, d], qb.at[z], base["q"] + z,
                dev(x, y, z_t, d), unless=jnp.logical_and(z_t == z, d == c),
            )
    remote(lamt.at[0], lamt.at[1], base["lam"], sib)
    mine_here = c == z // 2

    @pl.when(mine_here)
    def _():
        kv[x, z, c] = kvs[zl, pl.ds(pl.multiple_of(c * half_rows, half_rows), half_rows), :]
        for i in range(2):
            qb[z, i] = qs[zl, i, c]

    spread("up", True, [0])
    relay_z("up", 0)

    def relay_kv(k):
        zz = order[k]
        ref = kv.at[x, zz, c]
        got(ref, base["kvz"] + zz, mine_here if k == 0 else None)
        remote(ref, ref, base["kvx"] + zz, xnb)
        remote(ref, ref, base["kvs"] + zz, sib)

    for k in range(nz):
        relay_kv(k)
    for k in range(nz):
        got(qb.at[order[k]], base["q"] + order[k], mine_here if k == 0 else None)
    spread("dn", False)
    queries = qb[...].reshape(-1, width)
    first_lanes = lax.broadcasted_iota(jnp.int32, queries.shape, 1) < head_width
    zero = jnp.zeros_like(queries)
    qm[0] = jnp.where(first_lanes, queries, zero)
    qm[1] = jnp.where(first_lanes, zero, queries)
    tiles = top.shape[1]
    tile = queries.shape[0] // tiles

    def attend(xi, first):
        def body(qt, carry):
            block = kv[xi].reshape(-1, 2 * width)
            keys = block[:, :width]
            vals = block[:, width:]
            at = pl.ds(pl.multiple_of(qt * tile, tile), tile)
            for m in range(2):
                scores = lax.dot_general(
                    keys, qm[m, at, :], (((1,), (1,)), ((), ())), preferred_element_type=F32
                )
                peak = jnp.max(scores, axis=0, keepdims=True)
                if not first:
                    old = top[m, qt]
                    peak = jnp.maximum(old, peak)
                    shrink = jnp.exp(old - peak)
                e = jnp.exp(scores - peak)
                row = jnp.sum(e, axis=0, keepdims=True)
                acc = lax.dot_general(
                    vals, e.astype(BF), (((0,), (0,)), ((), ())), preferred_element_type=F32
                )
                if first:
                    top[m, qt] = peak
                else:
                    row += total[m, qt] * shrink
                    acc += summed[m, qt] * shrink
                total[m, qt] = row
                summed[m, qt] = acc
            return carry

        lax.fori_loop(0, tiles, body, 0)

    for k in range(nz):
        zz = order[k]
        got(kv.at[x, zz, 1 - c], base["kvs"] + zz)
    relay_z("dn", 0)
    attend(x, True)
    for k in range(nz):
        zz = order[k]
        ref = kv.at[1 - x, zz, c]
        got(ref, base["kvx"] + zz)
        remote(ref, ref, base["kvt"] + zz, sib)
    relay_x("up", 0)
    spread("up", True, [1])
    for k in range(nz):
        zz = order[k]
        got(kv.at[1 - x, zz, 1 - c], base["kvt"] + zz)
    attend(1 - x, False)

    there = 2 * (1 - y) + c
    got(lamt.at[1], base["lam"])
    weight = jnp.where(mine_here, lamt[0], lamt[1])[:1, :1]
    per = nz // tiles
    me = y * nz + z
    for qt in range(tiles):
        a = summed[0, qt] / total[0, qt]
        b = summed[1, qt] / total[1, qt]
        diff = a - weight * b
        norm = lax.rsqrt(jnp.mean(diff * diff, axis=0, keepdims=True) + 1e-05)
        done = ((diff * norm).T * hgain[...] * 0.8).astype(BF)
        hsrc[qt * per : (qt + 1) * per] = done.reshape((per,) + hsrc.shape[1:])
        for z_t in range(qt * per, (qt + 1) * per):
            for y_t in range(2):
                remote(
                    hsrc.at[z_t, y_t], hb.at[me], base["head"] + me, dev(x, y_t, z_t, c),
                    unless=jnp.logical_and(z == z_t, y == y_t),
                )
    hb[me] = hsrc[z, y]
    for k in range(1, nz):
        relay_z("up", k, [0])
    for i in range(2):
        got(ow_half(ow.at[there], i), base["ow"] + 2 + i)
        remote(ow_half(ow.at[there], i), ow_half(ow.at[there], i), base["ow"] + 4 + i, sib)
    for other in range(1, 2 * nz):
        k, dy = other % nz, other // nz
        src = ((y + dy) % 2) * nz + (z + k) % nz
        got(hb.at[src], base["head"] + src)
    loads[6].wait()
    for i in range(2):
        got(ow_half(ow.at[t + 1 - 2 * c], i), base["ow"] + i)
        got(ow_half(ow.at[there + 1 - 2 * c], i), base["ow"] + 4 + i)

    stream = res0[...].astype(F32)
    for tt in range(ow.shape[0]):
        pair = jnp.concatenate([hb[2 * tt], hb[2 * tt + 1]], axis=-1)
        stream += jnp.dot(pair, ow[tt], preferred_element_type=F32)
    center = stream - jnp.mean(stream, axis=-1, keepdims=True)
    spread_ = jnp.mean(center * center, axis=-1, keepdims=True)
    own = 2 * y + zl
    nb[own] = (center * lax.rsqrt(spread_ + 1e-05) * ngain[...]).astype(BF)
    zn = 2 * y + 1 - zl
    def nb_half(m, i):
        return nb.at[m, pl.ds(i * (piece // 2), piece // 2)]

    for i in range(2):
        remote(nb_half(own, i), nb_half(own, i), base["norm"] + i, znb)
        remote(nb_half(own, i), nb_half(own, i), base["norm"] + 2 + i, ynb)
    spread("dn", True, [0])
    for k in range(1, nz):
        relay_x("up", k, [0])
    for i in range(2):
        got(nb_half(zn, i), base["norm"] + i)
        remote(nb_half(zn, i), nb_half(zn, i), base["norm"] + 4 + i, ynb)
    for k in range(1, nz):
        relay_z("up", k, [1])
    spread("dn", True, [1])
    relay_x("dn", 0)
    for k in range(1, nz):
        relay_x("up", k, [1])
    for i in range(2):
        got(nb_half(2 * (1 - y) + zl, i), base["norm"] + 2 + i)
        got(nb_half(2 * (1 - y) + 1 - zl, i), base["norm"] + 4 + i)
    for k in range(nz):
        settle("up", k, False)
        settle("up", k, True)
    normed = nb[...].reshape(-1, nb.shape[2])
    lifted = None
    for zz in range(nz):
        for xx in range(2):
            at = (2 * zz + xx) * depth
            block = jnp.concatenate([up[xx, zz, p, d] for d in range(2) for p in range(P_)], axis=0)
            term = jnp.dot(normed[:, at : at + depth], block, preferred_element_type=F32)
            lifted = term if lifted is None else lifted + term
    lifted = jnp.maximum(lifted, 0.0)
    hidden[...] = (lifted * lifted).astype(BF)

    def lower(k, other, p):
        zz, xx = order[k], (1 - x if other else x)
        settle("dn", k, other, [p])
        i = (2 * zz + xx) * P_ + p
        r = jnp.dot(hidden[...], dn[xx, zz, p].reshape(units, -1), preferred_element_type=F32)
        r = r.reshape(mine.shape[1:])
        mine[i] = r
        part[i] = r.astype(BF)
        remote(part.at[i, pl.ds(2 * (1 - y), 2)], ygot.at[i], base["yg"] + i, ynb)
        return i

    def middle(i):
        got(ygot.at[i], base["yg"] + i)
        zsend[i] = (mine[i, zn] + ygot[i, 1 - zl].astype(F32)).astype(BF)
        remote(zsend.at[i], zgot.at[i], base["zg"] + i, znb)

    def finish(i):
        got(zgot.at[i], base["zg"] + i)
        span = mine.shape[3]
        at = pl.ds(pl.multiple_of(i * span, span), span)
        r = nb[own, :, at].astype(F32) + mine[i, own] + ygot[i, zl].astype(F32) + zgot[i].astype(F32)
        out[:, at] = r.astype(BF)

    done = []
    mid_at = 0
    for p in range(P_):
        for k in range(1, nz):
            relay_z("dn", k, [p])
        for k in range(nz):
            if k:
                relay_x("dn", k, [p])
            for other in (False, True):
                done.append(lower(k, other, p))
                if len(done) - mid_at > 2:
                    middle(done[mid_at])
                    mid_at += 1
    while mid_at < len(done):
        middle(done[mid_at])
        mid_at += 1
    for i in done:
        finish(i)
    for cp, unless in started:
        if unless is None:
            cp.wait_send()
        else:
            pl.when(jnp.logical_not(unless))(cp.wait_send)


def fused(n, nt, residual, first_query, second_query, first_key, second_key, values,
          lambdas, head_gain, out_weight, norm_gain, up_weight, down_weight):
    rows, width = first_query.shape
    heads = lambdas.shape[0]
    head_width = width // heads
    value_width = values.shape[1] // heads
    half = head_width // 2
    depth, units = up_weight.shape
    model = out_weight.shape[1]
    piece = residual.shape[0]
    nz = n // 2
    inverse = 10000.0 ** (-np.arange(half) * 2.0 / head_width)
    inverse = np.tile(inverse, 2 * heads)[None, :].astype(np.float32)
    vmem = pl.BlockSpec(memory_space=pltpu.VMEM)
    smem = pl.BlockSpec(memory_space=pltpu.SMEM)
    far = pl.BlockSpec(memory_space=pl.ANY)
    queries = rows * 2
    tiles = 2
    _, slots = receive_slots(nz)
    return pl.pallas_call(
        functools.partial(layer_kernel, nz, head_width),
        out_shape=jax.ShapeDtypeStruct((piece, model), BF),
        in_specs=[far] * 5 + [vmem, smem, vmem, far, vmem, vmem, far, far],
        out_specs=vmem,
        scratch_shapes=[
            pltpu.VMEM((2, rows, 2 * width), BF),
            pltpu.VMEM((2, 2, 2, piece, width), BF),
            pltpu.VMEM((2, nz, 2, rows // 2, 2 * width), BF),
            pltpu.VMEM((nz, 2, piece, width), BF),
            pltpu.VMEM((2, queries, width), BF),
            pltpu.VMEM((2, 8, 128), F32),
            pltpu.VMEM((nz, 2, piece, value_width), BF),
            pltpu.VMEM((2 * nz, piece, value_width), BF),
            pltpu.VMEM((2, nz, PIECES, 2, depth // (2 * PIECES), units), BF),
            pltpu.VMEM((2, nz, PIECES, 2, units // 2, depth // PIECES), BF),
            pltpu.VMEM((nt,) + out_weight.shape, BF),
            pltpu.VMEM((4, piece, model), BF),
            pltpu.VMEM((rows, units), BF),
            pltpu.VMEM((n * PIECES, 4, piece, depth // PIECES), F32),
            pltpu.VMEM((n * PIECES, 4, piece, depth // PIECES), BF),
            pltpu.VMEM((n * PIECES, 2, piece, depth // PIECES), BF),
            pltpu.VMEM((n * PIECES, piece, depth // PIECES), BF),
            pltpu.VMEM((n * PIECES, piece, depth // PIECES), BF),
            pltpu.VMEM((2, tiles, 1, queries // tiles), F32),
            pltpu.VMEM((2, tiles, 1, queries // tiles), F32),
            pltpu.VMEM((2, tiles, value_width, queries // tiles), F32),
            pltpu.SemaphoreType.DMA((400,)),
            pltpu.SemaphoreType.DMA((slots,)),
            pltpu.SemaphoreType.DMA((8,)),
        ] + [pltpu.VMEM((rows, width), BF)] * 4,
        compiler_params=pltpu.CompilerParams(
            collective_id=0, has_side_effects=True, vmem_limit_bytes=60 * 2**20
        ),
        name="layer",
    )(first_query, second_query, first_key, second_key, values, inverse,
      lambdas, head_gain.reshape(1, -1), out_weight, residual,
      norm_gain.reshape(1, -1), up_weight, down_weight)


def choose(*args):
    n, nt = lax.axis_size("sp"), lax.axis_size("tp")
    residual, query, values, lambdas, out_weight, up_weight = (
        args[0], args[1], args[5], args[6], args[8], args[10]
    )
    rows, width = query.shape
    heads = lambdas.shape[0]
    fits = 2 * n * 2 * up_weight.size * 2 // 2 + nt * out_weight.size * 2 <= VMEM_BUDGET
    square = nt == 4 and n == 2 * nt and heads == 2 and width == 128
    square = square and values.shape[1] == 2 * width and rows == nt * residual.shape[0]
    if square and fits and up_weight.shape[0] == rows:
        return fused(n, nt, *args)
    return local(*args)


def solution(mesh):
    in_specs = (
        P(("sp", "tp"), None),
        P("sp", "tp"),
        P("sp", "tp"),
        P("sp", "tp"),
        P("sp", "tp"),
        P("sp", "tp"),
        P("tp"),
        P(),
        P("tp", None),
        P(),
        P("sp", "tp"),
        P("tp", "sp"),
    )
    out_specs = P(("sp", "tp"), None)
    return jax.shard_map(choose, mesh=mesh, in_specs=in_specs, out_specs=out_specs, check_vma=False)
```

time: 113 us -> 105 us (0.929)
  the two profiles are of different devices: /device:TPU:0 before, /device:TPU:16 now
where the time goes in v1:
time: 105 us; the launch traced here: 104 us
  Pallas kernels  103 us (98%)
  local copies, waits for them, and re-layouts  1.67 us (2%)
    pallas_call x1, Pallas kernels, fused(): pl.pallas_call(functools.partial(layer_kernel, nz, head_width), out_shape...  103 us

profile of v1, /device:TPU:16, one launch (start us, length us, event | category | flops | bytes accessed | tf_op | source)
XLA Modules:
  0.0 104.5 jit_solution(13705201813668826555)
XLA Ops:
  0.0 102.8 %layer.1 = bf16[64,2048]{1,0:T(8,128)(2,1)} custom-call(bf16[256,128]{1,0:T(8,128)(2,1)} %qa_far.1, bf16[256,128]{1,0:T(8,128)(2,1)} %qb_far.1, bf16[256,128]{1,0:T(8,128)(2,1)} %ka_far.1, bf16[256,128]{1,0:T(8,128)(2,1)} %kb_far.1, bf16[256,256]{1,0:T(8,128)(2,1)} %v_far.1, f32[1,128]{1,0:T(1,128)} %constant.2.clone.inverse, f32[2]{0:T(128)} %lam.1, ...), custom_call_target="tpu_custom_call" | custom-call | tf_op jit(solution)/shard_map/layer/pallas_call | solution.py:560
  102.8 1.7 %copy.15 = bf16[64,2048]{1,0:T(8,128)(2,1)} copy(bf16[64,2048]{1,0:T(8,128)(2,1)} %layer.1) | data formatting | bytes 524288

commit v2 on v1

--- a/solution.py
+++ b/solution.py
@@ -156,13 +156,14 @@
     nz, head_width,
     qa_far, qb_far, ka_far, kb_far, v_far, inverse, lam, hgain, ow0, res0, ngain, up0, dn0,
     out,
-    kvs, qs, kv, qb, qm, lamt, hsrc, hb, up, dn, ow, nb, hidden, mine, part, ygot, zsend, zgot,
+    kvs, qs, kv, qb, qm, lamt, hsrc, hb, up, dn, ow, res, nb, hidden, mine, part, ygot, zsend, zgot,
     top, total, summed, send, recv, load, qa, qbb, ka, kb,
 ):
     s = lax.axis_index("sp")
     t = lax.axis_index("tp")
     z, x, y, c = s // 2, s % 2, t // 2, t % 2
-    zl = z % 2
+    zl, zh = z % 2, z // 2
+    pal = z + 1 - 2 * zl
     base, _ = receive_slots(nz)
     rows, width = ka.shape
     piece = res0.shape[0]
@@ -177,8 +178,8 @@
     sib = dev(x, y, z, 1 - c)
     xnb = dev(1 - x, y, z, c)
     ynb = dev(x, 1 - y, z, c)
-    znb = dev(x, y, z + 1 - 2 * zl, c)
-    order = [z, z + 1 - 2 * zl, (z + 2) % nz, nz - 1 - z]
+    znb = dev(x, y, pal, c)
+    order = [z, pal, (z + 2) % nz, nz - 1 - z]
 
     loads = [
         pltpu.make_async_copy(src, dst, load.at[i])
@@ -199,7 +200,7 @@
 
     started = []
 
-    def remote(src, dst, slot, peer, unless=None, local=False):
+    def remote(src, dst, slot, peer, unless=None):
         i = len(started)
         cp = pltpu.make_async_remote_copy(
             src_ref=src, dst_ref=dst, send_sem=send.at[i], recv_sem=recv.at[slot],
@@ -210,8 +211,6 @@
             cp.start()
         else:
             pl.when(jnp.logical_not(unless))(cp.start)
-            if local:
-                pl.when(unless)(pltpu.make_async_copy(src, dst, recv.at[slot]).start)
 
     def got(dst, slot, unless=None):
         cp = pltpu.make_async_remote_copy(
@@ -233,36 +232,28 @@
         size = buf.shape[4]
         span = buf.shape[5]
         for p in pieces:
-            for z_t in (c, c + 2):
-                for d in range(2):
-                    if name == "up":
-                        src = own.at[pl.ds((d * P_ + p) * size, size)]
-                    else:
-                        src = own.at[pl.ds(d * size, size), pl.ds(p * span, span)]
-                    dst = buf.at[x, z, p, d]
-                    slot = base[name + "z"] + z * P_ + p
-                    here = z_t == z
-                    skip = here if far else jnp.logical_not(here)
-                    if far:
-                        remote(src, dst, slot, dev(x, y, z_t, d), unless=here)
-                    else:
-                        i = len(started)
-                        cp = pltpu.make_async_remote_copy(
-                            src_ref=src, dst_ref=dst, send_sem=send.at[i], recv_sem=recv.at[slot],
-                            device_id=sib, device_id_type=MESH,
-                        )
-                        away = jnp.logical_or(skip, d == c)
-                        started.append((cp, away))
-                        pl.when(jnp.logical_not(away))(cp.start)
-                        near = jnp.logical_and(here, d == c)
-                        pl.when(near)(pltpu.make_async_copy(src, dst, recv.at[slot]).start)
+            for d in range(2):
+                if name == "up":
+                    src = own.at[pl.ds((d * P_ + p) * size, size)]
+                else:
+                    src = own.at[pl.ds(d * size, size), pl.ds(p * span, span)]
+                dst = buf.at[x, z, p, d]
+                slot = base[name + "z"] + z * P_ + p
+                if far:
+                    remote(src, dst, slot, dev(x, y, jnp.where(zl == c, (z + 2) % nz, 2 * (1 - zh) + c), d))
+                    remote(src, dst, slot, dev(x, y, pal, d), unless=zl == c)
+                else:
+                    remote(src, dst, slot, sib, unless=jnp.logical_or(zl != c, d == c))
+                    near = jnp.logical_and(zl == c, d == c)
+                    pl.when(near)(pltpu.make_async_copy(src, dst, recv.at[slot]).start)
 
     def relay_z(name, k, pieces=range(P_)):
         buf = weights[name][1]
         zz = order[k]
         for p in pieces:
             ref = buf.at[x, zz, p, c]
-            got(ref, base[name + "z"] + zz * P_ + p)
+            slot = base[name + "z"] + zz * P_ + p
+            got(ref, slot)
             remote(ref, ref, base[name + "x"] + zz * P_ + p, xnb)
             remote(ref, ref, base[name + "s"] + zz * P_ + p, sib)
 
@@ -302,48 +293,43 @@
         return first.astype(BF), second.astype(BF)
 
     lamt[0] = jnp.full(lamt.shape[1:], lam[zl], F32)
+    for cp in loads[:2]:
+        cp.wait()
+    for j, v in enumerate(packed(turn(ka), turn(kb))):
+        kvs[j, :, :width] = v
+    for cp in loads[2:4]:
+        cp.wait()
+    scale = head_width ** (-0.5)
+    for j, v in enumerate(packed(turn(qa), turn(qbb))):
+        qs[j] = (v.astype(F32) * scale).astype(BF).reshape(qs.shape[1:])
+    for cp in loads[4:6]:
+        cp.wait()
     pl.semaphore_wait(barrier, len(peers))
+    for j in range(2):
+        z_t = 2 * c + j
+        for d in range(2):
+            here = jnp.logical_and(z_t == z, d == c)
+            peer = dev(x, y, z_t, d)
+            src = kvs.at[j, pl.ds(d * half_rows, half_rows)]
+            remote(src, kv.at[x, z, d], base["kvz"] + z, peer, unless=here)
+    for j in range(2):
+        z_t = 2 * c + j
+        for d in range(2):
+            here = jnp.logical_and(z_t == z, d == c)
+            remote(qs.at[j, :, d], qb.at[zh, zl], base["q"] + z, dev(x, y, z_t, d), unless=here)
     spread("up", False)
     for i in range(2):
         remote(ow_half(ow0, i), ow_half(ow.at[t], i), base["ow"] + 2 + i, ynb)
     for i in range(2):
         remote(ow_half(ow0, i), ow_half(ow.at[t], i), base["ow"] + i, sib)
-    for cp in loads[:2]:
-        cp.wait()
-    for j, v in enumerate(packed(turn(ka), turn(kb))):
-        kvs[j, :, :width] = v
-    for cp in loads[4:6]:
-        cp.wait()
-    for j in range(2):
-        z_t = 2 * c + j
-        for d in range(2):
-            remote(
-                kvs.at[j, pl.ds(d * half_rows, half_rows)], kv.at[x, z, d], base["kvz"] + z,
-                dev(x, y, z_t, d), unless=jnp.logical_and(z_t == z, d == c),
-            )
-    for cp in loads[2:4]:
-        cp.wait()
-    scale = head_width ** (-0.5)
-    for j, v in enumerate(packed(turn(qa), turn(qbb))):
-        qs[j] = (v.astype(F32) * scale).astype(BF).reshape(qs.shape[1:])
-    for j in range(2):
-        z_t = 2 * c + j
-        for d in range(2):
-            remote(
-                qs.at[j, :, d], qb.at[z], base["q"] + z,
-                dev(x, y, z_t, d), unless=jnp.logical_and(z_t == z, d == c),
-            )
     remote(lamt.at[0], lamt.at[1], base["lam"], sib)
-    mine_here = c == z // 2
+    mine_here = c == zh
 
     @pl.when(mine_here)
     def _():
         kv[x, z, c] = kvs[zl, pl.ds(pl.multiple_of(c * half_rows, half_rows), half_rows), :]
         for i in range(2):
-            qb[z, i] = qs[zl, i, c]
-
-    spread("up", True, [0])
-    relay_z("up", 0)
+            qb[zh, zl, i] = qs[zl, i, c]
 
     def relay_kv(k):
         zz = order[k]
@@ -352,18 +338,18 @@
         remote(ref, ref, base["kvx"] + zz, xnb)
         remote(ref, ref, base["kvs"] + zz, sib)
 
-    for k in range(nz):
-        relay_kv(k)
-    for k in range(nz):
-        got(qb.at[order[k]], base["q"] + order[k], mine_here if k == 0 else None)
-    spread("dn", False)
-    queries = qb[...].reshape(-1, width)
-    first_lanes = lax.broadcasted_iota(jnp.int32, queries.shape, 1) < head_width
-    zero = jnp.zeros_like(queries)
-    qm[0] = jnp.where(first_lanes, queries, zero)
-    qm[1] = jnp.where(first_lanes, zero, queries)
+    def take_queries():
+        for k in range(nz):
+            zz = order[k]
+            got(qb.at[zz // 2, zz % 2], base["q"] + zz, mine_here if k == 0 else None)
+        queries = qb[...].reshape(-1, width)
+        first_lanes = lax.broadcasted_iota(jnp.int32, queries.shape, 1) < head_width
+        zero = jnp.zeros_like(queries)
+        qm[0] = jnp.where(first_lanes, queries, zero)
+        qm[1] = jnp.where(first_lanes, zero, queries)
+
     tiles = top.shape[1]
-    tile = queries.shape[0] // tiles
+    tile = qm.shape[1] // tiles
 
     def attend(xi, first):
         def body(qt, carry):
@@ -396,109 +382,114 @@
 
         lax.fori_loop(0, tiles, body, 0)
 
-    for k in range(nz):
-        zz = order[k]
-        got(kv.at[x, zz, 1 - c], base["kvs"] + zz)
-    relay_z("dn", 0)
-    attend(x, True)
-    for k in range(nz):
-        zz = order[k]
-        ref = kv.at[1 - x, zz, c]
-        got(ref, base["kvx"] + zz)
-        remote(ref, ref, base["kvt"] + zz, sib)
-    relay_x("up", 0)
-    spread("up", True, [1])
-    for k in range(nz):
-        zz = order[k]
-        got(kv.at[1 - x, zz, 1 - c], base["kvt"] + zz)
-    attend(1 - x, False)
+    def near_keys():
+        for k in range(nz):
+            got(kv.at[x, order[k], 1 - c], base["kvs"] + order[k])
+
+    def relay_keys(k):
+        ref = kv.at[1 - x, order[k], c]
+        got(ref, base["kvx"] + order[k])
+        remote(ref, ref, base["kvt"] + order[k], sib)
+
+    def far_keys():
+        for k in range(nz):
+            got(kv.at[1 - x, order[k], 1 - c], base["kvt"] + order[k])
 
     there = 2 * (1 - y) + c
-    got(lamt.at[1], base["lam"])
-    weight = jnp.where(mine_here, lamt[0], lamt[1])[:1, :1]
-    per = nz // tiles
     me = y * nz + z
-    for qt in range(tiles):
-        a = summed[0, qt] / total[0, qt]
-        b = summed[1, qt] / total[1, qt]
-        diff = a - weight * b
-        norm = lax.rsqrt(jnp.mean(diff * diff, axis=0, keepdims=True) + 1e-05)
-        done = ((diff * norm).T * hgain[...] * 0.8).astype(BF)
-        hsrc[qt * per : (qt + 1) * per] = done.reshape((per,) + hsrc.shape[1:])
-        for z_t in range(qt * per, (qt + 1) * per):
-            for y_t in range(2):
+
+    def finish_heads():
+        got(lamt.at[1], base["lam"])
+        weight = jnp.where(mine_here, lamt[0], lamt[1])[:1, :1]
+        for qt in range(tiles):
+            a = summed[0, qt] / total[0, qt]
+            b = summed[1, qt] / total[1, qt]
+            diff = a - weight * b
+            norm = lax.rsqrt(jnp.mean(diff * diff, axis=0, keepdims=True) + 1e-05)
+            hsrc[qt] = ((diff * norm).T * hgain[...] * 0.8).astype(BF)
+            for z_t in range(2 * qt, 2 * qt + 2):
                 remote(
-                    hsrc.at[z_t, y_t], hb.at[me], base["head"] + me, dev(x, y_t, z_t, c),
-                    unless=jnp.logical_and(z == z_t, y == y_t),
+                    hsrc.at[qt], hb.at[me], base["head"] + me, dev(x, y, z_t, c), unless=z == z_t,
                 )
-    hb[me] = hsrc[z, y]
-    for k in range(1, nz):
-        relay_z("up", k, [0])
-    for i in range(2):
-        got(ow_half(ow.at[there], i), base["ow"] + 2 + i)
-        remote(ow_half(ow.at[there], i), ow_half(ow.at[there], i), base["ow"] + 4 + i, sib)
-    for other in range(1, 2 * nz):
-        k, dy = other % nz, other // nz
-        src = ((y + dy) % 2) * nz + (z + k) % nz
-        got(hb.at[src], base["head"] + src)
-    loads[6].wait()
-    for i in range(2):
-        got(ow_half(ow.at[t + 1 - 2 * c], i), base["ow"] + i)
-        got(ow_half(ow.at[there + 1 - 2 * c], i), base["ow"] + 4 + i)
-
-    stream = res0[...].astype(F32)
-    for tt in range(ow.shape[0]):
-        pair = jnp.concatenate([hb[2 * tt], hb[2 * tt + 1]], axis=-1)
-        stream += jnp.dot(pair, ow[tt], preferred_element_type=F32)
-    center = stream - jnp.mean(stream, axis=-1, keepdims=True)
-    spread_ = jnp.mean(center * center, axis=-1, keepdims=True)
-    own = 2 * y + zl
-    nb[own] = (center * lax.rsqrt(spread_ + 1e-05) * ngain[...]).astype(BF)
-    zn = 2 * y + 1 - zl
-    def nb_half(m, i):
-        return nb.at[m, pl.ds(i * (piece // 2), piece // 2)]
-
-    for i in range(2):
-        remote(nb_half(own, i), nb_half(own, i), base["norm"] + i, znb)
-        remote(nb_half(own, i), nb_half(own, i), base["norm"] + 2 + i, ynb)
-    spread("dn", True, [0])
-    for k in range(1, nz):
-        relay_x("up", k, [0])
-    for i in range(2):
-        got(nb_half(zn, i), base["norm"] + i)
-        remote(nb_half(zn, i), nb_half(zn, i), base["norm"] + 4 + i, ynb)
-    for k in range(1, nz):
-        relay_z("up", k, [1])
-    spread("dn", True, [1])
-    relay_x("dn", 0)
-    for k in range(1, nz):
-        relay_x("up", k, [1])
-    for i in range(2):
-        got(nb_half(2 * (1 - y) + zl, i), base["norm"] + 2 + i)
-        got(nb_half(2 * (1 - y) + 1 - zl, i), base["norm"] + 4 + i)
-    for k in range(nz):
-        settle("up", k, False)
-        settle("up", k, True)
-    normed = nb[...].reshape(-1, nb.shape[2])
-    lifted = None
-    for zz in range(nz):
-        for xx in range(2):
-            at = (2 * zz + xx) * depth
-            block = jnp.concatenate([up[xx, zz, p, d] for d in range(2) for p in range(P_)], axis=0)
-            term = jnp.dot(normed[:, at : at + depth], block, preferred_element_type=F32)
-            lifted = term if lifted is None else lifted + term
-    lifted = jnp.maximum(lifted, 0.0)
-    hidden[...] = (lifted * lifted).astype(BF)
+        hb[me] = hsrc[zh]
+        remote(hb.at[me], hb.at[me], base["head"] + me, ynb)
+
+    def relay_heads(k):
+        at = y * nz + order[k]
+        got(hb.at[at], base["head"] + at)
+        remote(hb.at[at], hb.at[at], base["head"] + at, ynb)
+
+    def far_heads():
+        for k in range(nz):
+            at = (1 - y) * nz + order[k]
+            got(hb.at[at], base["head"] + at)
+
+    def relay_ow(i):
+        ref = ow_half(ow.at[there], i)
+        got(ref, base["ow"] + 2 + i)
+        remote(ref, ref, base["ow"] + 4 + i, sib)
+
+    own = 2 * zl + y
+    zn = 2 * (1 - zl) + y
+
+    def res_z():
+        remote(res0, res.at[own], base["norm"], znb)
+
+    def res_y():
+        remote(res0, res.at[own], base["norm"] + 1, ynb)
+
+    def relay_res():
+        got(res.at[zn], base["norm"])
+        remote(res.at[zn], res.at[zn], base["norm"] + 2, ynb)
+
+    def project():
+        loads[6].wait()
+        for i in range(2):
+            got(ow_half(ow.at[t + 1 - 2 * c], i), base["ow"] + i)
+            got(ow_half(ow.at[there + 1 - 2 * c], i), base["ow"] + 4 + i)
+        got(res.at[2 * zl + 1 - y], base["norm"] + 1)
+        got(res.at[2 * (1 - zl) + 1 - y], base["norm"] + 2)
+        res[own] = res0[...]
+
+        def body(i, carry):
+            at = pl.ds(pl.multiple_of(i * 2 * piece, 2 * piece), 2 * piece)
+            stream = res[pl.ds(2 * i, 2)].reshape(2 * piece, -1).astype(F32)
+            for tt in range(ow.shape[0]):
+                pair = jnp.concatenate([hb[2 * tt, at, :], hb[2 * tt + 1, at, :]], axis=-1)
+                stream += jnp.dot(pair, ow[tt], preferred_element_type=F32)
+            center = stream - jnp.mean(stream, axis=-1, keepdims=True)
+            spread_ = jnp.mean(center * center, axis=-1, keepdims=True)
+            row = (center * lax.rsqrt(spread_ + 1e-05) * ngain[...]).astype(BF)
+            nb[pl.ds(2 * i, 2)] = row.reshape(2, piece, -1)
+            return carry
+
+        lax.fori_loop(0, 2, body, 0)
+
+    def lift():
+        for k in range(nz):
+            settle("up", k, False)
+            settle("up", k, True)
+        normed = nb[...].reshape(-1, nb.shape[2])
+        lifted = None
+        for zz in range(nz):
+            for xx in range(2):
+                at = (2 * zz + xx) * depth
+                block = jnp.concatenate(
+                    [up[xx, zz, p, d] for d in range(2) for p in range(P_)], axis=0
+                )
+                term = jnp.dot(normed[:, at : at + depth], block, preferred_element_type=F32)
+                lifted = term if lifted is None else lifted + term
+        lifted = jnp.maximum(lifted, 0.0)
+        hidden[...] = (lifted * lifted).astype(BF)
 
     def lower(k, other, p):
         zz, xx = order[k], (1 - x if other else x)
         settle("dn", k, other, [p])
         i = (2 * zz + xx) * P_ + p
         r = jnp.dot(hidden[...], dn[xx, zz, p].reshape(units, -1), preferred_element_type=F32)
-        r = r.reshape(mine.shape[1:])
-        mine[i] = r
-        part[i] = r.astype(BF)
-        remote(part.at[i, pl.ds(2 * (1 - y), 2)], ygot.at[i], base["yg"] + i, ynb)
+        mine[i] = r.reshape(mine.shape[1:])
+        part[i] = r.astype(BF).reshape(part.shape[1:])
+        remote(part.at[i, :, 1 - y], ygot.at[i], base["yg"] + i, ynb)
         return i
 
     def middle(i):
@@ -514,21 +505,110 @@
         out[:, at] = r.astype(BF)
 
     done = []
-    mid_at = 0
-    for p in range(P_):
-        for k in range(1, nz):
-            relay_z("dn", k, [p])
-        for k in range(nz):
-            if k:
-                relay_x("dn", k, [p])
-            for other in (False, True):
-                done.append(lower(k, other, p))
-                if len(done) - mid_at > 2:
-                    middle(done[mid_at])
-                    mid_at += 1
-    while mid_at < len(done):
-        middle(done[mid_at])
-        mid_at += 1
+    passed = []
+
+    def low(k, other, p):
+        done.append(lower(k, other, p))
+
+    def mid():
+        i = done[len(passed)]
+        passed.append(i)
+        middle(i)
+
+    res_y()
+    relay_z("up", 0, [0])
+    relay_z("up", 0, [1])
+    res_z()
+    relay_kv(0)
+    relay_kv(1)
+    relay_kv(2)
+    relay_kv(3)
+    spread("up", True, [0])
+    spread("dn", False)
+    take_queries()
+    near_keys()
+    relay_z("dn", 0, [0])
+    relay_z("dn", 0, [1])
+    attend(x, True)
+    relay_keys(0)
+    relay_keys(1)
+    relay_keys(2)
+    relay_keys(3)
+    relay_x("up", 0, [0])
+    relay_x("up", 0, [1])
+    spread("up", True, [1])
+    far_keys()
+    attend(1 - x, False)
+    relay_res()
+    finish_heads()
+    relay_z("up", 1, [0])
+    relay_z("up", 2, [0])
+    relay_z("up", 3, [0])
+    relay_ow(0)
+    relay_heads(1)
+    relay_heads(2)
+    relay_heads(3)
+    relay_ow(1)
+    spread("dn", True, [0])
+    relay_x("up", 1, [0])
+    relay_x("up", 2, [0])
+    relay_x("up", 3, [0])
+    relay_z("up", 1, [1])
+    relay_z("up", 2, [1])
+    relay_z("up", 3, [1])
+    spread("dn", True, [1])
+    far_heads()
+    project()
+    relay_x("dn", 0, [0])
+    relay_x("dn", 0, [1])
+    relay_x("up", 1, [1])
+    relay_x("up", 2, [1])
+    relay_x("up", 3, [1])
+    relay_z("dn", 1, [0])
+    relay_z("dn", 2, [0])
+    relay_z("dn", 3, [0])
+    lift()
+    low(0, False, 0)
+    low(0, True, 0)
+    relay_x("dn", 1, [0])
+    relay_x("dn", 2, [0])
+    relay_x("dn", 3, [0])
+    low(1, False, 0)
+    mid()
+    low(1, True, 0)
+    mid()
+    relay_z("dn", 1, [1])
+    low(2, False, 0)
+    mid()
+    low(2, True, 0)
+    mid()
+    relay_z("dn", 2, [1])
+    low(3, False, 0)
+    mid()
+    low(3, True, 0)
+    mid()
+    relay_z("dn", 3, [1])
+    low(0, False, 1)
+    mid()
+    low(0, True, 1)
+    mid()
+    relay_x("dn", 1, [1])
+    low(1, False, 1)
+    mid()
+    low(1, True, 1)
+    mid()
+    relay_x("dn", 2, [1])
+    low(2, False, 1)
+    mid()
+    low(2, True, 1)
+    mid()
+    relay_x("dn", 3, [1])
+    low(3, False, 1)
+    mid()
+    low(3, True, 1)
+    mid()
+    mid()
+    mid()
     for i in done:
         finish(i)
     for cp, unless in started:
@@ -566,18 +646,19 @@
             pltpu.VMEM((2, rows, 2 * width), BF),
             pltpu.VMEM((2, 2, 2, piece, width), BF),
             pltpu.VMEM((2, nz, 2, rows // 2, 2 * width), BF),
-            pltpu.VMEM((nz, 2, piece, width), BF),
+            pltpu.VMEM((2, nz // 2, 2, piece, width), BF),
             pltpu.VMEM((2, queries, width), BF),
             pltpu.VMEM((2, 8, 128), F32),
-            pltpu.VMEM((nz, 2, piece, value_width), BF),
-            pltpu.VMEM((2 * nz, piece, value_width), BF),
+            pltpu.VMEM((2, rows, value_width), BF),
+            pltpu.VMEM((2 * nz, rows, value_width), BF),
             pltpu.VMEM((2, nz, PIECES, 2, depth // (2 * PIECES), units), BF),
             pltpu.VMEM((2, nz, PIECES, 2, units // 2, depth // PIECES), BF),
             pltpu.VMEM((nt,) + out_weight.shape, BF),
             pltpu.VMEM((4, piece, model), BF),
+            pltpu.VMEM((4, piece, model), BF),
             pltpu.VMEM((rows, units), BF),
             pltpu.VMEM((n * PIECES, 4, piece, depth // PIECES), F32),
-            pltpu.VMEM((n * PIECES, 4, piece, depth // PIECES), BF),
+            pltpu.VMEM((n * PIECES, 2, 2, piece, depth // PIECES), BF),
             pltpu.VMEM((n * PIECES, 2, piece, depth // PIECES), BF),
             pltpu.VMEM((n * PIECES, piece, depth // PIECES), BF),
             pltpu.VMEM((n * PIECES, piece, depth // PIECES), BF),

time: 105 us -> 90.8 us (0.86)
  the two profiles are of different devices: /device:TPU:16 before, /device:TPU:0 now
where the time goes in v2:
time: 90.8 us; the launch traced here: 90.6 us
  Pallas kernels  88.9 us (98%)
  local copies, waits for them, and re-layouts  1.67 us (2%)
    pallas_call x1, Pallas kernels, fused(): pl.pallas_call(functools.partial(layer_kernel, nz, head_width), out_shape...  88.9 us

profile of v2, /device:TPU:0, one launch (start us, length us, event | category | flops | bytes accessed | tf_op | source)
XLA Modules:
  0.0 90.6 jit_solution(17732155761755016515)
XLA Ops:
  0.0 88.9 %layer.1 = bf16[64,2048]{1,0:T(8,128)(2,1)} custom-call(bf16[256,128]{1,0:T(8,128)(2,1)} %qa_far.1, bf16[256,128]{1,0:T(8,128)(2,1)} %qb_far.1, bf16[256,128]{1,0:T(8,128)(2,1)} %ka_far.1, bf16[256,128]{1,0:T(8,128)(2,1)} %kb_far.1, bf16[256,256]{1,0:T(8,128)(2,1)} %v_far.1, f32[1,128]{1,0:T(1,128)} %constant.2.clone.inverse, f32[2]{0:T(128)} %lam.1, ...), custom_call_target="tpu_custom_call" | custom-call | tf_op jit(solution)/shard_map/layer/pallas_call | solution.py:640
  89.0 1.7 %copy.15 = bf16[64,2048]{1,0:T(8,128)(2,1)} copy(bf16[64,2048]{1,0:T(8,128)(2,1)} %layer.1) | data formatting | bytes 524288
